TPU v7x, 512 devices: a whole 4x4x16 slice. The times are simulated.
512 devices in a mesh: tp: 32 (over z, core), dp: 16 (over y, x).
Axes of the slice: x: 4, y: 4, z: 16, core: 2. Of those that a mesh axis runs over, the one named last changes fastest.
Arguments:
- tokens: bfloat16 [128, 4096], P('tp', 'dp'), may hold values from -6 to 6
- norm_gain: bfloat16 [2, 4096], P(None, 'dp'), may hold values from 0.099609375 to 1.8984375
- w_query: bfloat16 [2, 4096, 4096], P(None, 'dp', 'tp'), may hold values from -0.09375 to 0.09375
- w_key: bfloat16 [2, 4096, 4096], P(None, 'dp', 'tp'), may hold values from -0.09375 to 0.09375
- w_value: bfloat16 [2, 4096, 4096], P(None, 'dp', 'tp'), may hold values from -0.09375 to 0.09375
- w_outgate: bfloat16 [2, 4096, 4096], P(None, 'dp', 'tp'), may hold values from -0.09375 to 0.09375
- w_gates: bfloat16 [2, 4096, 64], P(None, 'dp'), may hold values from -0.09375 to 0.09375
- gate_bias: float32 [2, 2, 32], P(None, None, 'tp'), may hold values from -1 to 5
- w_out: bfloat16 [2, 4096, 4096], P(None, 'tp', 'dp'), may hold values from -0.09375 to 0.09375
- memory: float32 [2, 128, 32, 128, 128], P(None, 'dp', 'tp'), may hold values from -6 to 6
- normalizer: float32 [2, 128, 32, 128], P(None, 'dp', 'tp'), may hold values from -3 to 3
- stabilizer: float32 [2, 128, 32], P(None, 'dp', 'tp'), may hold values from -8 to 300, as said below
Outputs:
- mixed: bfloat16 [128, 4096], P('tp', 'dp')
- new_memory: float32 [2, 128, 32, 128, 128], P(None, 'dp', 'tp')
- new_normalizer: float32 [2, 128, 32, 128], P(None, 'dp', 'tp')
- new_stabilizer: float32 [2, 128, 32], P(None, 'dp', 'tp')
Inputs may be any that keep to these rules, and one draw needn't show every extreme that they name: `stabilizer`: lies between -8 and 8, except that some entries may be as large as 300.
All inputs are finite; a program needn't handle non-finite values.
Results may differ from a plain program's by a relative error of at most 0.04.
Values may be sent and summed in bfloat16 or wider, within the bound.
A program may use at most 64 MiB of HBM per device.

v0:
```python
import jax
import jax.numpy as jnp
from jax import lax
from jax.sharding import PartitionSpec as P

D = 4096
HEAD_SIZE = 128


epsilon = 1e-06


def cut_along(array, dim, devices):
    dims = array.shape
    parts = array.reshape(*dims[:dim], devices, dims[dim] // devices, *dims[dim + 1 :])
    return jnp.moveaxis(parts, dim, 0)


def summed_on_arrival(array, axis, dim):
    devices = lax.axis_size(axis)
    parts = lax.all_to_all(cut_along(array, dim, devices), axis, 0, 0, tiled=True)
    return jnp.sum(parts, axis=0)


def from_everyone(array, axis):
    copies = jnp.broadcast_to(array, (lax.axis_size(axis), *array.shape))
    return lax.all_to_all(copies, axis, split_axis=0, concat_axis=0, tiled=True)


def in_order(parts, dim):
    dims = list(parts.shape[1:])
    dims[dim] *= parts.shape[0]
    return jnp.moveaxis(parts, 0, dim).reshape(dims)


def gathered_copies(array, axis, dim):
    parts = from_everyone(array, axis)
    return in_order(parts, dim)


def sent_together(arrays, axis, dim, along):
    columns = [a.reshape(*a.shape[:along], -1) for a in arrays]
    both = jnp.concatenate(columns, axis=along)
    filled, at, done = (summed_on_arrival(both, axis, dim), 0, [])
    for a, column in zip(arrays, columns):
        slab = filled[..., at : at + column.shape[along]]
        done.append(slab.reshape(*slab.shape[:along], *a.shape[along:]))
        at += column.shape[along]
    return tuple(done)


def cell_update(query, key_rows, value_rows, input_pre, forget_pre, memory, normalizer, stabilizer):
    batch_size = query.shape[0]
    head_count = input_pre.shape[1]
    query_float = query.astype(jnp.float32).reshape(batch_size, head_count, -1)
    key_float = key_rows.astype(jnp.float32).reshape(
        batch_size, head_count, -1
    ) * query_float.shape[2] ** (-0.5)
    value_float = value_rows.astype(jnp.float32).reshape(batch_size, head_count, -1)
    carried = jax.nn.log_sigmoid(forget_pre) + stabilizer
    new_max = jnp.maximum(carried, input_pre)
    keep_factor = jnp.exp(carried - new_max)
    write_factor = jnp.exp(input_pre - new_max)
    new_memory = (
        keep_factor[:, :, None, None] * memory
        + write_factor[:, :, None, None] * value_float[:, :, :, None] * key_float[:, :, None, :]
    )
    new_normalizer = keep_factor[:, :, None] * normalizer + write_factor[:, :, None] * key_float
    numerator = jnp.sum(new_memory * query_float[:, :, None, :], axis=3)
    denominator = jnp.sum(new_normalizer * query_float, axis=2)
    floor_value = jnp.maximum(jnp.abs(denominator), jnp.exp(-new_max))
    readout = numerator / jnp.maximum(floor_value, 1.0)[:, :, None]
    return (readout.reshape(batch_size, -1), new_memory, new_normalizer, new_max)


def finish_split(partial_out, wide_rows):
    summed = summed_on_arrival(partial_out, "tp", 0)
    own_rows = lax.dynamic_slice_in_dim(
        wide_rows, lax.axis_index("tp") * summed.shape[0], summed.shape[0], 0
    )
    return (own_rows + summed).astype(jnp.bfloat16)


def body(
    tokens,
    norm_gain,
    w_query,
    w_key,
    w_value,
    w_outgate,
    w_gates,
    gate_bias,
    w_out,
    memory,
    normalizer,
    stabilizer,
):
    heads_here = w_query.shape[2] // HEAD_SIZE
    all_heads = w_gates.shape[2] // 2
    head_first = lax.axis_index("tp") * heads_here
    current = tokens
    gathered = None
    memories = []
    normalizers = []
    maxima = []
    for layer_index in range(2):
        gathered = gathered_copies(current, "tp", 0)
        wide_rows = gathered.astype(jnp.float32)
        square_part = jnp.sum(wide_rows * wide_rows, axis=1)
        scaled = (wide_rows * norm_gain[layer_index].astype(jnp.float32)[None, :]).astype(
            jnp.bfloat16
        )
        gate_weight = w_gates[layer_index]
        own_gates = jnp.concatenate(
            [
                lax.dynamic_slice_in_dim(gate_weight, head_first, heads_here, 1),
                lax.dynamic_slice_in_dim(gate_weight, all_heads + head_first, heads_here, 1),
            ],
            axis=1,
        )
        term_query = jnp.dot(scaled, w_query[layer_index], preferred_element_type=jnp.float32)
        term_key = jnp.dot(scaled, w_key[layer_index], preferred_element_type=jnp.float32)
        term_value = jnp.dot(scaled, w_value[layer_index], preferred_element_type=jnp.float32)
        term_outgate = jnp.dot(scaled, w_outgate[layer_index], preferred_element_type=jnp.float32)
        term_gates = jnp.dot(scaled, own_gates, preferred_element_type=jnp.float32)
        sum_query, sum_key, sum_value, sum_outgate, sum_gates, square_own = sent_together(
            (term_query, term_key, term_value, term_outgate, term_gates, square_part), "dp", 0, 1
        )
        inv_scale = lax.rsqrt(square_own / D + epsilon)[:, None]
        query = (sum_query * inv_scale).astype(jnp.bfloat16)
        key_rows = (sum_key * inv_scale).astype(jnp.bfloat16)
        value_rows = (sum_value * inv_scale).astype(jnp.bfloat16)
        outgate = (sum_outgate * inv_scale).astype(jnp.bfloat16)
        gate_pre = sum_gates * inv_scale
        bias_here = gate_bias[layer_index]
        input_pre = gate_pre[:, :heads_here] + bias_here[0][None, :]
        forget_pre = gate_pre[:, heads_here:] + bias_here[1][None, :]
        readout, new_memory, new_normalizer, new_max = cell_update(
            query,
            key_rows,
            value_rows,
            input_pre,
            forget_pre,
            memory[layer_index],
            normalizer[layer_index],
            stabilizer[layer_index],
        )
        gated = (jax.nn.sigmoid(outgate.astype(jnp.float32)) * readout).astype(jnp.bfloat16)
        out_weight = w_out[layer_index]
        partial_out = jnp.dot(
            gathered_copies(gated, "dp", 0), out_weight, preferred_element_type=jnp.float32
        )
        if layer_index == 0:
            current = finish_split(partial_out, wide_rows)
            gathered = None
        else:
            current = finish_split(partial_out, wide_rows)
        memories.append(new_memory)
        normalizers.append(new_normalizer)
        maxima.append(new_max)
    return (current, jnp.stack(memories), jnp.stack(normalizers), jnp.stack(maxima))


def solution(mesh):
    placed = (
        P("tp", "dp"),
        P(None, "dp"),
        P(None, "dp", "tp"),
        P(None, "dp", "tp"),
        P(None, "dp", "tp"),
        P(None, "dp", "tp"),
        P(None, "dp", None),
        P(None, None, "tp"),
        P(None, "tp", "dp"),
        P(None, "dp", "tp", None, None),
        P(None, "dp", "tp", None),
        P(None, "dp", "tp"),
    )
    return jax.shard_map(
        body,
        mesh=mesh,
        in_specs=placed,
        out_specs=(
            P("tp", "dp"),
            P(None, "dp", "tp", None, None),
            P(None, "dp", "tp", None),
            P(None, "dp", "tp"),
        ),
        check_vma=False,
    )
```

profile of v0, /device:TPU:1, one launch (start us, length us, event | category | flops | bytes accessed | tf_op | source)
XLA Modules:
  0.0 158.1 jit_solution(5264320394995219169)
XLA Ops:
  0.6 1.3 broadcast_in_dim.8
  2.0 16.9 %all-to-all-start = ((bf16[32,4,256]{2,1,0:T(4,128)(2,1)}), bf16[32,4,256]{2,1,0:T(4,128)(2,1)S(1)}, u32[]{:S(2)}, u32[]{:S(2)}) async-start(bf16[32,4,256]{2,1,0:T(4,128)(2,1)} %broadcast_in_dim.8), calls=%async_computation | async-start | bytes 131072 | tf_op jit(solution)/shard_map/all_to_all | solution.py:27
  18.9 0.6 copy-done.8
  19.6 12.3 %all-to-all-done = bf16[32,4,256]{2,1,0:T(4,128)(2,1)S(1)} async-done(((bf16[32,4,256]{2,1,0:T(4,128)(2,1)}), bf16[32,4,256]{2,1,0:T(4,128)(2,1)S(1)}, u32[]{:S(2)}, u32[]{:S(2)}) %all-to-all-start) | async-done | bytes 65568 | tf_op jit(solution)/shard_map/all_to_all | solution.py:27
  32.1 0.8 copy-done.1
  32.9 0.1 fusion.20
  33.1 0.1 fusion.22
  33.2 0.7 copy-done.3
  34.0 0.1 fusion.24
  34.1 0.8 copy-done.4
  34.9 0.1 fusion.26
  35.2 0.8 concatenate.20
  36.0 6.9 %all-to-all-start.1 = ((f32[16,8,515]{2,1,0:T(8,128)}), f32[16,8,515]{2,1,0:T(8,128)S(1)}, u32[]{:S(2)}, u32[]{:S(2)}) async-start(f32[16,8,515]{2,1,0:T(8,128)} %concatenate.20), calls=%async_computation.1 | async-start | bytes 655360 | tf_op jit(solution)/shard_map/all_to_all | solution.py:21
  43.0 0.7 fusion.89
  43.7 7.3 %all-to-all-done.1 = f32[16,8,515]{2,1,0:T(8,128)S(1)} async-done(((f32[16,8,515]{2,1,0:T(8,128)}), f32[16,8,515]{2,1,0:T(8,128)S(1)}, u32[]{:S(2)}, u32[]{:S(2)}) %all-to-all-start.1) | async-done | bytes 263712 | tf_op jit(solution)/shard_map/all_to_all | solution.py:21
  51.0 0.2 fusion.62
  51.3 1.5 exponential_reduce_fusion.3
  52.9 0.2 multiply_reduce_fusion.3
  53.3 0.4 fusion.5
  53.8 9.1 %all_to_all.40 = bf16[16,8,128]{2,1,0:T(8,128)(2,1)S(1)} all-to-all(bf16[16,8,128]{2,1,0:T(8,128)(2,1)S(1)} %broadcast_in_dim.9), channel_id=1, replica_groups=mesh['tp'=32,'dp'=16] {'dp'}, dimensions={0} | all-to-all | bytes 65536 | tf_op jit(solution)/shard_map/all_to_all | solution.py:27
  63.1 0.8 copy.77
  63.8 7.7 %all-to-all-start.3 = ((f32[32,4,256]{2,1,0:T(4,128)}), f32[32,4,256]{2,1,0:T(4,128)S(1)}, u32[]{:S(2)}, u32[]{:S(2)}) async-start(f32[32,4,256]{2,1,0:T(4,128)} %copy.77), calls=%async_computation.3 | async-start | bytes 262144 | tf_op jit(solution)/shard_map/all_to_all | solution.py:21
  71.6 16.2 %all-to-all-done.3 = f32[32,4,256]{2,1,0:T(4,128)S(1)} async-done(((f32[32,4,256]{2,1,0:T(4,128)}), f32[32,4,256]{2,1,0:T(4,128)S(1)}, u32[]{:S(2)}, u32[]{:S(2)}) %all-to-all-start.3) | async-done | bytes 131104 | tf_op jit(solution)/shard_map/all_to_all | solution.py:21
  87.8 0.6 broadcast_in_dim.10
  88.5 4.8 %all-to-all-start.4 = ((bf16[32,4,256]{2,1,0:T(4,128)(2,1)}), bf16[32,4,256]{2,1,0:T(4,128)(2,1)S(1)}, u32[]{:S(2)}, u32[]{:S(2)}) async-start(bf16[32,4,256]{2,1,0:T(4,128)(2,1)} %broadcast_in_dim.10), calls=%async_computation.4 | async-start | bytes 131072 | tf_op jit(solution)/shard_map/all_to_all | solution.py:27
  93.3 13.0 %all-to-all-done.4 = bf16[32,4,256]{2,1,0:T(4,128)(2,1)S(1)} async-done(((bf16[32,4,256]{2,1,0:T(4,128)(2,1)}), bf16[32,4,256]{2,1,0:T(4,128)(2,1)S(1)}, u32[]{:S(2)}, u32[]{:S(2)}) %all-to-all-start.4) | async-done | bytes 65568 | tf_op jit(solution)/shard_map/all_to_all | solution.py:27
  106.5 0.1 fusion.10
  106.6 0.2 fusion.12
  106.8 0.2 fusion.14
  106.9 0.2 fusion.16
  107.3 0.8 concatenate.23
  108.2 3.5 %all-to-all-start.5 = ((f32[16,8,515]{2,1,0:T(8,128)}), f32[16,8,515]{2,1,0:T(8,128)S(1)}, u32[]{:S(2)}, u32[]{:S(2)}) async-start(f32[16,8,515]{2,1,0:T(8,128)} %concatenate.23), calls=%async_computation.5 | async-start | bytes 655360 | tf_op jit(solution)/shard_map/all_to_all | solution.py:21
  111.8 7.8 %all-to-all-done.5 = f32[16,8,515]{2,1,0:T(8,128)S(1)} async-done(((f32[16,8,515]{2,1,0:T(8,128)}), f32[16,8,515]{2,1,0:T(8,128)S(1)}, u32[]{:S(2)}, u32[]{:S(2)}) %all-to-all-start.5) | async-done | bytes 263712 | tf_op jit(solution)/shard_map/all_to_all | solution.py:21
  119.6 0.2 fusion.54
  119.9 1.6 exponential_reduce_fusion.1
  121.5 0.2 multiply_reduce_fusion.2
  121.9 0.4 fusion.2
  122.4 0.6 broadcast_in_dim.11
  123.1 3.5 %all-to-all-start.6 = ((bf16[16,8,128]{2,1,0:T(8,128)(2,1)}), bf16[16,8,128]{2,1,0:T(8,128)(2,1)S(1)}, u32[]{:S(2)}, u32[]{:S(2)}) async-start(bf16[16,8,128]{2,1,0:T(8,128)(2,1)} %broadcast_in_dim.11), calls=%async_computation.6 | async-start | bytes 65536 | tf_op jit(solution)/shard_map/all_to_all | solution.py:27
  126.6 0.6 pad_maximum_fusion.1
  127.2 5.8 %all-to-all-done.6 = bf16[16,8,128]{2,1,0:T(8,128)(2,1)S(1)} async-done(((bf16[16,8,128]{2,1,0:T(8,128)(2,1)}), bf16[16,8,128]{2,1,0:T(8,128)(2,1)S(1)}, u32[]{:S(2)}, u32[]{:S(2)}) %all-to-all-start.6) | async-done | bytes 32800 | tf_op jit(solution)/shard_map/all_to_all | solution.py:27
  133.1 0.7 copy.84
  133.8 7.5 %all-to-all-start.7 = ((f32[32,4,256]{2,1,0:T(4,128)}), f32[32,4,256]{2,1,0:T(4,128)S(1)}, u32[]{:S(2)}, u32[]{:S(2)}) async-start(f32[32,4,256]{2,1,0:T(4,128)} %copy.84), calls=%async_computation.7 | async-start | bytes 262144 | tf_op jit(solution)/shard_map/all_to_all | solution.py:21
  141.3 0.6 pad_maximum_fusion.2
  141.9 0.4 multiply_add_fusion.1
  142.3 1.0 pad_maximum_fusion
  143.3 14.2 %all-to-all-done.7 = f32[32,4,256]{2,1,0:T(4,128)S(1)} async-done(((f32[32,4,256]{2,1,0:T(4,128)}), f32[32,4,256]{2,1,0:T(4,128)S(1)}, u32[]{:S(2)}, u32[]{:S(2)}) %all-to-all-start.7) | async-done | bytes 131104 | tf_op jit(solution)/shard_map/all_to_all | solution.py:21
  157.5 0.6 add_convert_fusion
  (59 shorter events, 2.4 us)
Async XLA Ops:
  2.0 16.9 %copy-start.6 = (bf16[2,256,64]{1,2,0:T(8,128)(2,1)S(1)}, bf16[2,256,64]{1,2,0:T(8,128)(2,1)}, u32[]{:S(2)}) copy-start(bf16[2,256,64]{1,2,0:T(8,128)(2,1)} %param.18) | copy-start | bytes 196612
  2.0 29.9 %all-to-all-start = ((bf16[32,4,256]{2,1,0:T(4,128)(2,1)}), bf16[32,4,256]{2,1,0:T(4,128)(2,1)S(1)}, u32[]{:S(2)}, u32[]{:S(2)}) async-start(bf16[32,4,256]{2,1,0:T(4,128)(2,1)} %broadcast_in_dim.8), calls=%async_computation | async-start | bytes 131072 | tf_op jit(solution)/shard_map/all_to_all | solution.py:27
  18.9 0.7 copy-start.8
  32.0 0.9 copy-start.1
  32.1 1.0 copy-start.2
  33.0 0.9 copy-start.3
  34.0 0.9 copy-start.4
  35.0 18.3 %copy-start = (f32[2,8,1,128,128]{4,3,2,1,0:T(8,128)S(1)}, f32[2,8,1,128,128]{4,3,2,1,0:T(8,128)}, u32[]{:S(2)}) copy-start(f32[2,8,1,128,128]{4,3,2,1,0:T(8,128)} %param.21) | copy-start | bytes 3145732
  36.0 6.9 %copy-start.10 = (f32[2,8,1]{1,2,0:T(1,128)S(1)}, f32[2,8,1]{1,2,0:T(1,128)}, u32[]{:S(2)}) copy-start(f32[2,8,1]{1,2,0:T(1,128)} %param.23) | copy-start | bytes 196
  36.0 7.0 %copy-start.9 = (f32[2,2,1]{1,2,0:T(1,128)S(1)}, f32[2,2,1]{1,2,0:T(1,128)}, u32[]{:S(2)}) copy-start(f32[2,2,1]{1,2,0:T(1,128)} %param.19) | copy-start | bytes 52
  36.0 15.0 %all-to-all-start.1 = ((f32[16,8,515]{2,1,0:T(8,128)}), f32[16,8,515]{2,1,0:T(8,128)S(1)}, u32[]{:S(2)}, u32[]{:S(2)}) async-start(f32[16,8,515]{2,1,0:T(8,128)} %concatenate.20), calls=%async_computation.1 | async-start | bytes 655360 | tf_op jit(solution)/shard_map/all_to_all | solution.py:21
  51.3 1.5 copy-start.7
  53.3 9.6 %copy-start.5 = (bf16[2,128,256]{2,1,0:T(8,128)(2,1)S(1)}, bf16[2,128,256]{2,1,0:T(8,128)(2,1)}, u32[]{:S(2)}) copy-start(bf16[2,128,256]{2,1,0:T(8,128)(2,1)} %param.20) | copy-start | bytes 393220
  63.8 23.9 %all-to-all-start.3 = ((f32[32,4,256]{2,1,0:T(4,128)}), f32[32,4,256]{2,1,0:T(4,128)S(1)}, u32[]{:S(2)}, u32[]{:S(2)}) async-start(f32[32,4,256]{2,1,0:T(4,128)} %copy.77), calls=%async_computation.3 | async-start | bytes 262144 | tf_op jit(solution)/shard_map/all_to_all | solution.py:21
  88.5 17.9 %all-to-all-start.4 = ((bf16[32,4,256]{2,1,0:T(4,128)(2,1)}), bf16[32,4,256]{2,1,0:T(4,128)(2,1)S(1)}, u32[]{:S(2)}, u32[]{:S(2)}) async-start(bf16[32,4,256]{2,1,0:T(4,128)(2,1)} %broadcast_in_dim.10), calls=%async_computation.4 | async-start | bytes 131072 | tf_op jit(solution)/shard_map/all_to_all | solution.py:27
  108.2 11.4 %all-to-all-start.5 = ((f32[16,8,515]{2,1,0:T(8,128)}), f32[16,8,515]{2,1,0:T(8,128)S(1)}, u32[]{:S(2)}, u32[]{:S(2)}) async-start(f32[16,8,515]{2,1,0:T(8,128)} %concatenate.23), calls=%async_computation.5 | async-start | bytes 655360 | tf_op jit(solution)/shard_map/all_to_all | solution.py:21
  123.1 9.9 %all-to-all-start.6 = ((bf16[16,8,128]{2,1,0:T(8,128)(2,1)}), bf16[16,8,128]{2,1,0:T(8,128)(2,1)S(1)}, u32[]{:S(2)}, u32[]{:S(2)}) async-start(bf16[16,8,128]{2,1,0:T(8,128)(2,1)} %broadcast_in_dim.11), calls=%async_computation.6 | async-start | bytes 65536 | tf_op jit(solution)/shard_map/all_to_all | solution.py:27
  133.8 23.7 %all-to-all-start.7 = ((f32[32,4,256]{2,1,0:T(4,128)}), f32[32,4,256]{2,1,0:T(4,128)S(1)}, u32[]{:S(2)}, u32[]{:S(2)}) async-start(f32[32,4,256]{2,1,0:T(4,128)} %copy.84), calls=%async_computation.7 | async-start | bytes 262144 | tf_op jit(solution)/shard_map/all_to_all | solution.py:21
where the time goes:
time: 159 us; the launch traced here: 158 us
  waiting for transfers between devices  76.5 us (48%)
  starting transfers between devices  50.8 us (32%)
  local copies, waits for them, and re-layouts  10 us (6%)
  blocking collectives  9.1 us (6%)
  other arithmetic  8.98 us (6%)
  matrix products  1.74 us (1%)
    all_to_all x4, waiting for transfers between devices, summed_on_arrival(): lax.all_to_all(cut_along(array, dim, devices), axis, 0, 0, tiled=True)  45.4 us
    all_to_all x3, waiting for transfers between devices, from_everyone(): return lax.all_to_all(copies, axis, split_axis=0, concat_axis=0, tiled=True)  31.1 us
    all_to_all x4, starting transfers between devices, summed_on_arrival(): lax.all_to_all(cut_along(array, dim, devices), axis, 0, 0, tiled=True)  25.6 us
    all_to_all x3, starting transfers between devices, from_everyone(): return lax.all_to_all(copies, axis, split_axis=0, concat_axis=0, tiled=True)  25.2 us
    all_to_all x1, blocking collectives, from_everyone(): return lax.all_to_all(copies, axis, split_axis=0, concat_axis=0, tiled=True)  9.1 us
  transfers between devices with their start and end apart: 7, of which 7 were waited for; matrix products, arithmetic and copies ran while one was open for 2% of the time, Pallas kernels for 0%

commit v1 on v0

v1 whole, which is shorter than its diff:
```python
import functools
import math

import jax
import jax.numpy as jnp
from jax import lax
from jax.experimental import pallas as pl
from jax.experimental.pallas import tpu as pltpu
from jax.sharding import PartitionSpec as P

HEAD = 128
ROWS = 8
EPS = 1e-06
MESH = pl.DeviceIdType.MESH
F32 = jnp.float32
BF16 = jnp.bfloat16


def ring_order(n):
    return sorted(range(1, n), key=lambda d: -min(d, n - d))


def plane_order(side):
    pairs = [(a, b) for a in range(side) for b in range(side) if a or b]
    return sorted(pairs, key=lambda t: -(min(t[0], side - t[0]) + min(t[1], side - t[1])))


def kernel(
    ntp,
    ndp,
    tok_h,
    gain_h,
    wq_h,
    wk_h,
    wv_h,
    wo_h,
    wg_h,
    bias_h,
    wout_h,
    mem_h,
    nrm_h,
    stab_h,
    mixed_o,
    mem_o,
    nrm_o,
    stab_o,
    tok_v,
    gain_v,
    w_v,
    wg_v,
    bias_v,
    wout_v,
    mem_v,
    memb_v,
    nrm_v,
    stab_v,
    xg,
    bsend,
    brecv,
    cg,
    dsend,
    drecv,
    small_sem,
    w_sem,
    wout_sem,
    mem_sem,
    out_sem,
    swap_sem,
    send_sem,
    recv_sem,
):
    nz = ntp // 2
    side = math.isqrt(ndp)
    width = ndp * 256
    all_heads = ntp
    tp = lax.axis_index("tp")
    dp = lax.axis_index("dp")
    z = tp // 2
    c = lax.rem(tp, 2)
    y = dp // side
    x = lax.rem(dp, side)

    def z_at(dz, flip):
        nc = 1 - c if flip else c
        return lax.rem(z + dz, nz) * 2 + nc

    def dp_at(dy, dx):
        return lax.rem(y + dy, side) * side + lax.rem(x + dx, side)

    partner = z * 2 + 1 - c
    z_near = [(dz, flip) for dz in ring_order(nz) for flip in (0, 1)]
    plane = plane_order(side)

    small = [
        pltpu.make_async_copy(tok_h, tok_v, small_sem.at[0]),
        pltpu.make_async_copy(gain_h, gain_v, small_sem.at[1]),
        pltpu.make_async_copy(wg_h, wg_v, small_sem.at[2]),
        pltpu.make_async_copy(bias_h, bias_v, small_sem.at[3]),
        pltpu.make_async_copy(nrm_h, nrm_v, small_sem.at[4]),
        pltpu.make_async_copy(stab_h, stab_v, small_sem.at[5]),
    ]
    for copy in small:
        copy.start()
    weights = []
    for i, ref in enumerate((wq_h, wk_h, wv_h, wo_h)):
        weights.append(
            pltpu.make_async_copy(ref, w_v.at[:, :, pl.ds(i * HEAD, HEAD)], w_sem.at[i])
        )
    for copy in weights:
        copy.start()
    own_out = wout_v.at[:, pl.ds(pl.multiple_of(c * HEAD, HEAD), HEAD)]
    load_out = pltpu.make_async_copy(wout_h, own_out, wout_sem)
    load_out.start()
    load_mem = pltpu.make_async_copy(mem_h, mem_v, mem_sem)
    load_mem.start()

    barrier = pltpu.get_barrier_semaphore()
    greeted = 0
    for dz, flip in z_near:
        pl.semaphore_signal(
            barrier, 1, device_id={"tp": z_at(dz, flip), "dp": dp}, device_id_type=MESH
        )
        greeted += 1
    for dy, dx in plane:
        for other in (tp, partner):
            pl.semaphore_signal(
                barrier, 1, device_id={"tp": other, "dp": dp_at(dy, dx)}, device_id_type=MESH
            )
            greeted += 1
    pl.semaphore_signal(barrier, 1, device_id={"tp": partner, "dp": dp}, device_id_type=MESH)
    greeted += 1

    for copy in small:
        copy.wait()
    row8 = lax.broadcasted_iota(jnp.int32, (1, ROWS, 128), 1)
    upper = row8 < 4
    lane = lax.broadcasted_iota(jnp.int32, (1, 128), 1)
    row_of = lax.broadcasted_iota(jnp.int32, (ROWS, 128), 0)

    wide = tok_v[...].astype(F32)
    own_x = jnp.concatenate([wide[:, :128], wide[:, 128:]], axis=0)
    xg[0, tp] = own_x.astype(BF16)

    source = lax.broadcasted_iota(jnp.int32, (2 * all_heads, 128), 0)
    target = lax.broadcasted_iota(jnp.int32, (2 * all_heads, 128), 1)
    pick = ((target == 0) & (source == tp)) | ((target == 1) & (source == all_heads + tp))
    one_hot = jnp.where(pick, 1.0, 0.0).astype(BF16)
    for layer in range(2):
        w_v[layer, :, 4 * HEAD :] = jnp.dot(
            wg_v[layer], one_hot, preferred_element_type=F32
        ).astype(BF16)
    load_out.wait()
    load_mem.wait()
    for copy in weights:
        copy.wait()
    memb_v[...] = mem_v[...].astype(BF16)

    pl.semaphore_wait(barrier, greeted)

    def send(src, dst, layer, phase, to_tp, to_dp):
        pltpu.make_async_remote_copy(
            src_ref=src,
            dst_ref=dst,
            send_sem=send_sem.at[layer, phase],
            recv_sem=recv_sem.at[layer, phase],
            device_id={"tp": to_tp, "dp": to_dp},
            device_id_type=MESH,
        ).start()

    def all_of(ref, sem):
        pltpu.make_async_copy(ref, ref, sem).wait()

    def share_x(layer):
        for dz, flip in z_near:
            send(xg.at[layer, tp], xg.at[layer, tp], layer, 0, z_at(dz, flip), dp)
        send(xg.at[layer, tp], xg.at[layer, tp], layer, 0, partner, dp)

    share_x(0)
    swap = pltpu.make_async_remote_copy(
        src_ref=own_out,
        dst_ref=own_out,
        send_sem=swap_sem.at[0],
        recv_sem=swap_sem.at[1],
        device_id={"tp": partner, "dp": dp},
        device_id_type=MESH,
    )
    swap.start()

    for layer in range(2):
        all_of(xg.at[layer, pl.ds(0, ntp - 1)], recv_sem.at[layer, 0])
        tiles = xg[layer].astype(F32).reshape(nz, 2, ROWS, 128)
        even, odd = tiles[:, 0], tiles[:, 1]
        low = jnp.where(upper, even, pltpu.roll(odd, 4, 1)).reshape(nz * ROWS, 128)
        high = jnp.where(upper, pltpu.roll(even, 4, 1), odd).reshape(nz * ROWS, 128)
        squares = jnp.sum(low * low + high * high, axis=1, keepdims=True)
        gain = gain_v[pl.ds(layer, 1), :].astype(F32)
        scaled = jnp.concatenate(
            [(low * gain[:, :128]).astype(BF16), (high * gain[:, 128:]).astype(BF16)], axis=1
        )
        terms = jnp.dot(scaled, w_v[layer], preferred_element_type=F32)
        gates = jnp.where(lane == 2, squares, terms[:, 4 * HEAD :])
        gates_high = gates.astype(BF16).astype(F32)
        gates_low = pltpu.roll(gates - gates_high, 3, 1)
        gates = jnp.where(lane < 3, gates_high, gates_low)
        bsend[layer] = (
            jnp.concatenate([terms[:, : 4 * HEAD], gates], axis=1)
            .astype(BF16)
            .reshape(ndp, ROWS, 5 * HEAD)
        )
        for dy, dx in plane:
            to = dp_at(dy, dx)
            send(bsend.at[layer, to], brecv.at[layer, dp], layer, 1, tp, to)
        brecv[layer, dp] = bsend[layer, dp]
        all_of(brecv.at[layer, pl.ds(0, ndp - 1)], recv_sem.at[layer, 1])

        sums = jnp.sum(brecv[layer].astype(F32), axis=0)
        extra = sums[:, 4 * HEAD :]
        extra = extra + pltpu.roll(extra, 125, 1)
        inv = lax.rsqrt(extra[:, 2:3] / width + EPS)
        query = (sums[:, :HEAD] * inv).astype(BF16)
        key = (sums[:, HEAD : 2 * HEAD] * inv).astype(BF16).astype(F32) * HEAD**-0.5
        value = (sums[:, 2 * HEAD : 3 * HEAD] * inv).astype(BF16).astype(F32)
        outgate = (sums[:, 3 * HEAD : 4 * HEAD] * inv).astype(BF16).astype(F32)
        input_pre = extra[:, 0:1] * inv + bias_v[layer, 0:1, :]
        forget_pre = extra[:, 1:2] * inv + bias_v[layer, 1:2, :]
        log_forget = jnp.minimum(forget_pre, 0.0) - jnp.log1p(jnp.exp(-jnp.abs(forget_pre)))
        carried = log_forget + stab_v[layer]
        new_max = jnp.maximum(carried, input_pre)
        keep = jnp.exp(carried - new_max)
        write = jnp.exp(input_pre - new_max)
        query_float = query.astype(F32)
        read = jnp.zeros((ROWS, HEAD), F32)
        for s in range(ROWS):
            one = jnp.where(row_of == s, query_float, 0.0).astype(BF16)
            read = read + lax.dot_general(
                one, memb_v[layer, s], (((1,), (1,)), ((), ())), preferred_element_type=F32
            )
        match = jnp.sum(key * query_float, axis=1, keepdims=True)
        numerator = keep * read + (write * match) * value
        normalizer = keep * nrm_v[layer] + write * key
        denominator = jnp.sum(normalizer * query_float, axis=1, keepdims=True)
        floor = jnp.maximum(jnp.maximum(jnp.abs(denominator), jnp.exp(-new_max)), 1.0)
        gated = (jax.nn.sigmoid(outgate) * (numerator / floor)).astype(BF16)
        slot = c * ndp + dp
        cg[layer, slot] = gated
        for dy, dx in plane:
            for other in (tp, partner):
                send(cg.at[layer, slot], cg.at[layer, slot], layer, 2, other, dp_at(dy, dx))
        send(cg.at[layer, slot], cg.at[layer, slot], layer, 2, partner, dp)

        nrm_v[layer] = normalizer
        stab_v[layer] = new_max
        value_columns = jnp.transpose(write * value)
        for s in range(ROWS):
            mem_v[layer, s] = (
                keep[s : s + 1, :] * mem_v[layer, s]
                + value_columns[:, s : s + 1] * key[s : s + 1, :]
            )
        pltpu.make_async_copy(mem_v.at[layer], mem_o.at[layer], out_sem.at[layer]).start()

        all_of(cg.at[layer, pl.ds(0, ntp - 1)], recv_sem.at[layer, 2])
        if layer == 0:
            swap.wait()
        heads = cg[layer].reshape(2, ndp * ROWS, 128)
        both = jnp.concatenate([heads[0], heads[1]], axis=1)
        product = jnp.dot(both, wout_v[layer], preferred_element_type=F32)
        left = product[:, :128].reshape(ndp, ROWS, 128)
        right = product[:, 128:].reshape(ndp, ROWS, 128)
        for_even = jnp.where(upper, left, pltpu.roll(right, 4, 1))
        for_odd = jnp.where(upper, pltpu.roll(left, 4, 1), right)
        mine = jnp.where(c == 0, for_even, for_odd)
        dsend[layer] = mine.astype(BF16)
        for dz in ring_order(nz):
            to = lax.rem(z + dz, nz)
            send(dsend.at[layer, to], drecv.at[layer, z], layer, 3, to * 2 + c, dp)
        drecv[layer, z] = dsend[layer, z]
        all_of(drecv.at[layer, pl.ds(0, nz - 1)], recv_sem.at[layer, 3])
        own_x = (own_x + jnp.sum(drecv[layer].astype(F32), axis=0)).astype(BF16)
        if layer == 0:
            xg[1, tp] = own_x
            own_x = own_x.astype(F32)
            share_x(1)

    wide = own_x.astype(F32)
    tok_v[...] = jnp.concatenate([wide[:4], wide[4:]], axis=1).astype(BF16)
    outs = [
        pltpu.make_async_copy(tok_v, mixed_o, small_sem.at[0]),
        pltpu.make_async_copy(nrm_v, nrm_o, small_sem.at[1]),
        pltpu.make_async_copy(stab_v, stab_o, small_sem.at[2]),
    ]
    for copy in outs:
        copy.start()
    for layer in range(2):
        all_of(xg.at[layer, pl.ds(0, ntp - 1)], send_sem.at[layer, 0])
        all_of(brecv.at[layer, pl.ds(0, ndp - 1)], send_sem.at[layer, 1])
        all_of(cg.at[layer, pl.ds(0, ntp - 1)], send_sem.at[layer, 2])
        all_of(drecv.at[layer, pl.ds(0, nz - 1)], send_sem.at[layer, 3])
        pltpu.make_async_copy(mem_v.at[layer], mem_o.at[layer], out_sem.at[layer]).wait()
    for copy in outs:
        copy.wait()


def body(ntp, ndp, *args):
    tokens, gain, wq, wk, wv, wo, wg, bias, wout, memory, normalizer, stabilizer = args
    nz = ntp // 2
    hbm = pl.BlockSpec(memory_space=pltpu.HBM)
    memory = memory.reshape(2, ROWS, HEAD, HEAD)
    normalizer = normalizer.reshape(2, ROWS, HEAD)
    out = pl.pallas_call(
        functools.partial(kernel, ntp, ndp),
        out_shape=(
            jax.ShapeDtypeStruct(tokens.shape, BF16),
            jax.ShapeDtypeStruct(memory.shape, F32),
            jax.ShapeDtypeStruct(normalizer.shape, F32),
            jax.ShapeDtypeStruct(stabilizer.shape, F32),
        ),
        in_specs=[hbm] * 12,
        out_specs=(hbm,) * 4,
        scratch_shapes=[
            pltpu.VMEM(tokens.shape, BF16),
            pltpu.VMEM(gain.shape, BF16),
            pltpu.VMEM((2, 256, 5 * HEAD), BF16),
            pltpu.VMEM(wg.shape, BF16),
            pltpu.VMEM(bias.shape, F32),
            pltpu.VMEM((2, 2 * HEAD, 256), BF16),
            pltpu.VMEM(memory.shape, F32),
            pltpu.VMEM(memory.shape, BF16),
            pltpu.VMEM(normalizer.shape, F32),
            pltpu.VMEM(stabilizer.shape, F32),
            pltpu.VMEM((2, ntp, ROWS, 128), BF16),
            pltpu.VMEM((2, ndp, ROWS, 5 * HEAD), BF16),
            pltpu.VMEM((2, ndp, ROWS, 5 * HEAD), BF16),
            pltpu.VMEM((2, 2 * ndp, ROWS, 128), BF16),
            pltpu.VMEM((2, nz, ROWS, 128), BF16),
            pltpu.VMEM((2, nz, ROWS, 128), BF16),
            pltpu.SemaphoreType.DMA((6,)),
            pltpu.SemaphoreType.DMA((4,)),
            pltpu.SemaphoreType.DMA,
            pltpu.SemaphoreType.DMA,
            pltpu.SemaphoreType.DMA((2,)),
            pltpu.SemaphoreType.DMA((2,)),
            pltpu.SemaphoreType.DMA((2, 4)),
            pltpu.SemaphoreType.DMA((2, 4)),
        ],
        compiler_params=pltpu.CompilerParams(collective_id=0, has_side_effects=True),
    )(tokens, gain, wq, wk, wv, wo, wg, bias, wout, memory, normalizer, stabilizer)
    mixed, new_memory, new_normalizer, new_stabilizer = out
    return (
        mixed,
        new_memory.reshape(2, ROWS, 1, HEAD, HEAD),
        new_normalizer.reshape(2, ROWS, 1, HEAD),
        new_stabilizer,
    )


def solution(mesh):
    placed = (
        P("tp", "dp"),
        P(None, "dp"),
        P(None, "dp", "tp"),
        P(None, "dp", "tp"),
        P(None, "dp", "tp"),
        P(None, "dp", "tp"),
        P(None, "dp", None),
        P(None, None, "tp"),
        P(None, "tp", "dp"),
        P(None, "dp", "tp", None, None),
        P(None, "dp", "tp", None),
        P(None, "dp", "tp"),
    )
    return jax.shard_map(
        functools.partial(body, mesh.shape["tp"], mesh.shape["dp"]),
        mesh=mesh,
        in_specs=placed,
        out_specs=(
            P("tp", "dp"),
            P(None, "dp", "tp", None, None),
            P(None, "dp", "tp", None),
            P(None, "dp", "tp"),
        ),
        check_vma=False,
    )
```

time: 159 us -> 76.8 us (0.48)
  waiting for transfers between devices: 76.5 us -> 0 us
  Pallas kernels: 0 us -> 67.4 us
  starting transfers between devices: 50.8 us -> 0 us
  blocking collectives: 9.1 us -> 0 us
  other arithmetic: 8.98 us -> 0 us
  matrix products: 1.74 us -> 0 us
    all_to_all x7 -> x0, waiting for transfers between devices: 76.5 us -> none  [the longest x4 45.4 us: summed_on_arrival(): lax.all_to_all(cut_along(array, dim, devices), axis, 0, 0, tiled=True)]
    pallas_call x0 -> x1, Pallas kernels: none -> 67.4 us  [body(): pl.pallas_call(functools.partial(kernel, ntp, ndp), out_shape=(jax.ShapeD...]
    all_to_all x7 -> x0, starting transfers between devices: 50.8 us -> none  [the longest x4 25.6 us: summed_on_arrival(): lax.all_to_all(cut_along(array, dim, devices), axis, 0, 0, tiled=True)]
    all_to_all x1 -> x0, blocking collectives: 9.1 us -> none  [from_everyone(): return lax.all_to_all(copies, axis, split_axis=0, concat_axis=0, tiled=True)]
    unnamed x22 -> x17, local copies, waits for them, and re-layouts: 2.98 us -> 8.47 us
    exp x2 -> x0, other arithmetic: 3.08 us -> none  [cell_update(): keep_factor = jnp.exp(carried - new_max)]
    broadcast_in_dim x4 -> x0, local copies, waits for them, and re-layouts: 2.62 us -> none  [from_everyone(): copies = jnp.broadcast_to(array, (lax.axis_size(axis), *array.shape))]
    another operation x5 -> x0, other arithmetic: 2.36 us -> none  [the longest x1 1.04 us: body(): jnp.stack(memories)]
  transfers between devices with their start and end apart: 7 -> 0, of which waited for: 7 -> 0; matrix products, arithmetic and copies ran while one was open for 2% -> 0% of each run, Pallas kernels for 0% -> 0%
where the time goes in v1:
time: 76.8 us; the launch traced here: 76.5 us
  Pallas kernels  67.4 us (88%)
  local copies, waits for them, and re-layouts  8.47 us (11%)
    pallas_call x1, Pallas kernels, body(): pl.pallas_call(functools.partial(kernel, ntp, ndp), out_shape=(jax.ShapeD...  67.4 us
    unnamed x17, local copies, waits for them, and re-layouts  8.47 us

profile of v1, /device:TPU:1, one launch (start us, length us, event | category | flops | bytes accessed | tf_op | source)
XLA Modules:
  0.0 76.5 jit_solution(5361577422568905326)
XLA Ops:
  0.6 0.0 copy-start.3
  0.6 0.7 copy-done.3
  1.3 0.0 copy-start.4
  1.3 0.7 copy.17.bias_h
  2.0 0.0 copy-done.4
  2.0 0.7 copy.18.stab_h
  2.7 1.6 %copy.16.wg_h = bf16[2,256,64]{2,1,0:T(8,128)(2,1)} copy(bf16[2,256,64]{1,2,0:T(8,128)(2,1)} %param.18) | data formatting | bytes 131072 | tf_op args[6]
  4.3 67.4 %shard_map.147 = (bf16[4,256]{1,0:T(4,128)(2,1)}, f32[2,8,128,128]{3,2,1,0:T(8,128)}, f32[2,8,128]{2,1,0:T(8,128)}, f32[2,8,1]{2,1,0:T(8,128)}) custom-call(bf16[4,256]{1,0:T(4,128)(2,1)} %tok_h.1, bf16[2,256]{1,0:T(2,128)(2,1)} %gain_h.1, bf16[2,256,128]{2,1,0:T(8,128)(2,1)} %wq_h.1, bf16[2,256,128]{2,1,0:T(8,128)(2,1)} %wk_h.1, bf16[2,256,128]{2,1,0:T(8,128)(2,1)} %wv_h.1, ...), custom_call_target="tpu_custom_call" | custom-call | tf_op jit(solution)/shard_map/pallas_call | solution.py:309
  71.6 0.0 copy-start
  71.7 0.7 copy-done
  72.3 0.0 copy-start.2
  72.3 0.6 copy.21
  73.0 0.0 copy-done.2
  73.0 0.6 copy.25
  73.6 0.0 copy-start.1
  73.6 2.3 %copy.26 = f32[2,8,1,128,128]{4,3,2,1,0:T(8,128)} copy(f32[2,8,1,128,128]{4,3,2,1,0:T(8,128)} %bitcast.9) | data formatting | bytes 2097152
  75.9 0.0 copy-done.1
  75.9 0.6 copy.27
Async XLA Ops:
  0.6 0.7 copy-start.3
  1.3 0.7 copy-start.4
  71.6 0.7 copy-start
  72.3 0.7 copy-start.2
  73.6 2.3 %copy-start.1 = (f32[2,8,128]{2,1,0:T(8,128)S(1)}, f32[2,8,128]{2,1,0:T(8,128)}, u32[]{:S(2)}) copy-start(f32[2,8,128]{2,1,0:T(8,128)} %get-tuple-element.10) | copy-start | bytes 24580

commit v2 on v1

--- a/solution.py
+++ b/solution.py
@@ -11,6 +11,7 @@
 HEAD = 128
 ROWS = 8
 EPS = 1e-06
+GROUPS = ((0, 1), (1, 2), (2, 4), (4, 16))
 MESH = pl.DeviceIdType.MESH
 F32 = jnp.float32
 BF16 = jnp.bfloat16
@@ -55,19 +56,22 @@
     nrm_v,
     stab_v,
     xg,
+    x1g,
     bsend,
     brecv,
     cg,
     dsend,
     drecv,
+    last_send,
+    last_recv,
     small_sem,
     w_sem,
     wout_sem,
     mem_sem,
-    out_sem,
     swap_sem,
     send_sem,
     recv_sem,
+    group_sem,
 ):
     nz = ntp // 2
     side = math.isqrt(ndp)
@@ -130,39 +134,26 @@
     pl.semaphore_signal(barrier, 1, device_id={"tp": partner, "dp": dp}, device_id_type=MESH)
     greeted += 1
 
-    for copy in small:
-        copy.wait()
     row8 = lax.broadcasted_iota(jnp.int32, (1, ROWS, 128), 1)
     upper = row8 < 4
     lane = lax.broadcasted_iota(jnp.int32, (1, 128), 1)
     row_of = lax.broadcasted_iota(jnp.int32, (ROWS, 128), 0)
-
+    diagonal = lax.broadcasted_iota(jnp.int32, (ROWS, ROWS), 0) == lax.broadcasted_iota(
+        jnp.int32, (ROWS, ROWS), 1
+    )
+
+    small[0].wait()
     wide = tok_v[...].astype(F32)
     own_x = jnp.concatenate([wide[:, :128], wide[:, 128:]], axis=0)
-    xg[0, tp] = own_x.astype(BF16)
-
-    source = lax.broadcasted_iota(jnp.int32, (2 * all_heads, 128), 0)
-    target = lax.broadcasted_iota(jnp.int32, (2 * all_heads, 128), 1)
-    pick = ((target == 0) & (source == tp)) | ((target == 1) & (source == all_heads + tp))
-    one_hot = jnp.where(pick, 1.0, 0.0).astype(BF16)
-    for layer in range(2):
-        w_v[layer, :, 4 * HEAD :] = jnp.dot(
-            wg_v[layer], one_hot, preferred_element_type=F32
-        ).astype(BF16)
-    load_out.wait()
-    load_mem.wait()
-    for copy in weights:
-        copy.wait()
-    memb_v[...] = mem_v[...].astype(BF16)
-
+    xg[tp] = own_x.astype(BF16)
     pl.semaphore_wait(barrier, greeted)
 
-    def send(src, dst, layer, phase, to_tp, to_dp):
+    def send(src, dst, layer, phase, to_tp, to_dp, arrival=None):
         pltpu.make_async_remote_copy(
             src_ref=src,
             dst_ref=dst,
             send_sem=send_sem.at[layer, phase],
-            recv_sem=recv_sem.at[layer, phase],
+            recv_sem=recv_sem.at[layer, phase] if arrival is None else arrival,
             device_id={"tp": to_tp, "dp": to_dp},
             device_id_type=MESH,
         ).start()
@@ -170,12 +161,10 @@
     def all_of(ref, sem):
         pltpu.make_async_copy(ref, ref, sem).wait()
 
-    def share_x(layer):
-        for dz, flip in z_near:
-            send(xg.at[layer, tp], xg.at[layer, tp], layer, 0, z_at(dz, flip), dp)
-        send(xg.at[layer, tp], xg.at[layer, tp], layer, 0, partner, dp)
-
-    share_x(0)
+    for dz, flip in z_near:
+        send(xg.at[tp], xg.at[tp], 0, 0, z_at(dz, flip), dp)
+    send(xg.at[tp], xg.at[tp], 0, 0, partner, dp)
+    load_out.wait()
     swap = pltpu.make_async_remote_copy(
         src_ref=own_out,
         dst_ref=own_out,
@@ -186,10 +175,36 @@
     )
     swap.start()
 
+    for copy in small[1:]:
+        copy.wait()
+    for copy in weights:
+        copy.wait()
+    source = lax.broadcasted_iota(jnp.int32, (2 * all_heads, 128), 0)
+    target = lax.broadcasted_iota(jnp.int32, (2 * all_heads, 128), 1)
+    pick = ((target == 0) & (source == tp)) | ((target == 1) & (source == all_heads + tp))
+    one_hot = jnp.where(pick, 1.0, 0.0).astype(BF16)
     for layer in range(2):
-        all_of(xg.at[layer, pl.ds(0, ntp - 1)], recv_sem.at[layer, 0])
-        tiles = xg[layer].astype(F32).reshape(nz, 2, ROWS, 128)
-        even, odd = tiles[:, 0], tiles[:, 1]
+        w_v[layer, :, 4 * HEAD :] = lax.dot_general(
+            wg_v[layer], one_hot, (((0,), (0,)), ((), ())), preferred_element_type=F32
+        ).astype(BF16)
+    load_mem.wait()
+    memb_v[...] = mem_v[...].astype(BF16)
+    stab_columns = [
+        jnp.sum(jnp.where(diagonal, stab_v[layer], 0.0), axis=1, keepdims=True)
+        for layer in range(2)
+    ]
+
+    for layer in range(2):
+        if layer == 0:
+            all_of(xg.at[pl.ds(0, ntp - 1)], recv_sem.at[0, 0])
+            tiles = xg[...].astype(F32).reshape(nz, 2, ROWS, 128)
+            even, odd = tiles[:, 0], tiles[:, 1]
+        else:
+            all_of(drecv.at[pl.ds(0, nz - 1)], recv_sem.at[1, 0])
+            tiles = x1g[...].astype(F32)
+            even, odd = (
+                jnp.concatenate([tiles[:, core, 0], tiles[:, core, 1]], axis=0) for core in (0, 1)
+            )
         low = jnp.where(upper, even, pltpu.roll(odd, 4, 1)).reshape(nz * ROWS, 128)
         high = jnp.where(upper, pltpu.roll(even, 4, 1), odd).reshape(nz * ROWS, 128)
         squares = jnp.sum(low * low + high * high, axis=1, keepdims=True)
@@ -221,10 +236,10 @@
         key = (sums[:, HEAD : 2 * HEAD] * inv).astype(BF16).astype(F32) * HEAD**-0.5
         value = (sums[:, 2 * HEAD : 3 * HEAD] * inv).astype(BF16).astype(F32)
         outgate = (sums[:, 3 * HEAD : 4 * HEAD] * inv).astype(BF16).astype(F32)
-        input_pre = extra[:, 0:1] * inv + bias_v[layer, 0:1, :]
-        forget_pre = extra[:, 1:2] * inv + bias_v[layer, 1:2, :]
+        input_pre = extra[:, 0:1] * inv + bias_v[layer, :, 0:1]
+        forget_pre = extra[:, 1:2] * inv + bias_v[layer, :, 1:2]
         log_forget = jnp.minimum(forget_pre, 0.0) - jnp.log1p(jnp.exp(-jnp.abs(forget_pre)))
-        carried = log_forget + stab_v[layer]
+        carried = log_forget + stab_columns[layer]
         new_max = jnp.maximum(carried, input_pre)
         keep = jnp.exp(carried - new_max)
         write = jnp.exp(input_pre - new_max)
@@ -243,60 +258,105 @@
         gated = (jax.nn.sigmoid(outgate) * (numerator / floor)).astype(BF16)
         slot = c * ndp + dp
         cg[layer, slot] = gated
+        arrival = None
+        if layer == 1:
+            group = sum(jnp.where(dp >= first, 1, 0) for first, _ in GROUPS[1:])
+            arrival = group_sem.at[group]
         for dy, dx in plane:
             for other in (tp, partner):
-                send(cg.at[layer, slot], cg.at[layer, slot], layer, 2, other, dp_at(dy, dx))
-        send(cg.at[layer, slot], cg.at[layer, slot], layer, 2, partner, dp)
-
-        nrm_v[layer] = normalizer
-        stab_v[layer] = new_max
+                to = dp_at(dy, dx)
+                send(cg.at[layer, slot], cg.at[layer, slot], layer, 2, other, to, arrival)
+        send(cg.at[layer, slot], cg.at[layer, slot], layer, 2, partner, dp, arrival)
+
+        nrm_o[layer] = normalizer
+        stab_o[layer] = jnp.sum(jnp.where(diagonal, new_max, 0.0), axis=0, keepdims=True)
         value_columns = jnp.transpose(write * value)
         for s in range(ROWS):
-            mem_v[layer, s] = (
+            mem_o[layer, s] = (
                 keep[s : s + 1, :] * mem_v[layer, s]
                 + value_columns[:, s : s + 1] * key[s : s + 1, :]
             )
-        pltpu.make_async_copy(mem_v.at[layer], mem_o.at[layer], out_sem.at[layer]).start()
-
-        all_of(cg.at[layer, pl.ds(0, ntp - 1)], recv_sem.at[layer, 2])
+
+        def projected(first, last):
+            count = last - first
+            heads = [
+                cg[layer, pl.ds(core * ndp + first, count)].reshape(count * ROWS, 128)
+                for core in (0, 1)
+            ]
+            both = jnp.concatenate(heads, axis=1)
+            product = jnp.dot(both, wout_v[layer], preferred_element_type=F32)
+            left = product[:, :128].reshape(count, ROWS, 128)
+            right = product[:, 128:].reshape(count, ROWS, 128)
+            for_even = jnp.where(upper, left, pltpu.roll(right, 4, 1))
+            for_odd = jnp.where(upper, pltpu.roll(left, 4, 1), right)
+            return jnp.where(c == 0, for_even, for_odd).astype(BF16)
+
+        half = nz // 2
         if layer == 0:
+            all_of(cg.at[layer, pl.ds(0, ntp - 1)], recv_sem.at[layer, 2])
             swap.wait()
-        heads = cg[layer].reshape(2, ndp * ROWS, 128)
-        both = jnp.concatenate([heads[0], heads[1]], axis=1)
-        product = jnp.dot(both, wout_v[layer], preferred_element_type=F32)
-        left = product[:, :128].reshape(ndp, ROWS, 128)
-        right = product[:, 128:].reshape(ndp, ROWS, 128)
-        for_even = jnp.where(upper, left, pltpu.roll(right, 4, 1))
-        for_odd = jnp.where(upper, pltpu.roll(left, 4, 1), right)
-        mine = jnp.where(c == 0, for_even, for_odd)
-        dsend[layer] = mine.astype(BF16)
-        for dz in ring_order(nz):
-            to = lax.rem(z + dz, nz)
-            send(dsend.at[layer, to], drecv.at[layer, z], layer, 3, to * 2 + c, dp)
-        drecv[layer, z] = dsend[layer, z]
-        all_of(drecv.at[layer, pl.ds(0, nz - 1)], recv_sem.at[layer, 3])
-        own_x = (own_x + jnp.sum(drecv[layer].astype(F32), axis=0)).astype(BF16)
-        if layer == 0:
-            xg[1, tp] = own_x
-            own_x = own_x.astype(F32)
-            share_x(1)
+            mine = projected(0, ndp)
+            dsend[:, 0] = mine[:half]
+            dsend[:, 1] = mine[half:]
+            pair = lax.rem(z, half)
+            for dz in ring_order(nz):
+                to = lax.rem(z + dz, nz)
+                send(dsend.at[lax.rem(to, half)], drecv.at[z], 0, 3, to * 2 + c, dp)
+            drecv[z] = dsend[pair]
+            before = jnp.stack([xg[2 * pair + c], xg[2 * (pair + half) + c]]).astype(F32)
+            all_of(drecv.at[pl.ds(0, nz - 1)], recv_sem.at[0, 3])
+            x1g[pair, c] = (before + jnp.sum(drecv[...].astype(F32), axis=0)).astype(BF16)
+            mine_at = x1g.at[pair, c]
+            for dz in sorted(range(1 - nz // 4, nz // 4 + 1), key=lambda d: -abs(d)):
+                for flip in (0, 1):
+                    if dz or flip:
+                        send(mine_at, mine_at, 1, 0, z_at(dz + nz, flip), dp)
+            own_x = x1g[pair, c, z // half].astype(F32)
+        else:
+            for index, (first, last) in enumerate(GROUPS):
+                count = 2 * (last - first)
+                inside = (dp >= first) & (dp < last)
+
+                @pl.when(inside)
+                def _():
+                    all_of(cg.at[1, pl.ds(0, count - 1)], group_sem.at[index])
+
+                @pl.when(jnp.logical_not(inside))
+                def _():
+                    all_of(cg.at[1, pl.ds(0, count)], group_sem.at[index])
+
+                last_send[first:last] = projected(first, last)
+                for to in range(first, last):
+
+                    @pl.when(z != to)
+                    def _():
+                        send(last_send.at[to], last_recv.at[z], 1, 3, to * 2 + c, dp)
+
+            last_recv[z] = last_send[z]
+            all_of(last_recv.at[pl.ds(0, nz - 1)], recv_sem.at[1, 3])
+            own_x = (own_x + jnp.sum(last_recv[...].astype(F32), axis=0)).astype(BF16)
 
     wide = own_x.astype(F32)
-    tok_v[...] = jnp.concatenate([wide[:4], wide[4:]], axis=1).astype(BF16)
-    outs = [
-        pltpu.make_async_copy(tok_v, mixed_o, small_sem.at[0]),
-        pltpu.make_async_copy(nrm_v, nrm_o, small_sem.at[1]),
-        pltpu.make_async_copy(stab_v, stab_o, small_sem.at[2]),
-    ]
-    for copy in outs:
-        copy.start()
+    mixed_o[...] = jnp.concatenate([wide[:4], wide[4:]], axis=1).astype(BF16)
+    all_of(xg.at[pl.ds(0, ntp - 1)], send_sem.at[0, 0])
+    all_of(drecv.at[pl.ds(0, nz - 1)], send_sem.at[1, 0])
+    all_of(drecv.at[pl.ds(0, nz - 1)], send_sem.at[0, 3])
+    all_of(last_recv.at[pl.ds(0, nz - 1)], send_sem.at[1, 3])
     for layer in range(2):
-        all_of(xg.at[layer, pl.ds(0, ntp - 1)], send_sem.at[layer, 0])
         all_of(brecv.at[layer, pl.ds(0, ndp - 1)], send_sem.at[layer, 1])
         all_of(cg.at[layer, pl.ds(0, ntp - 1)], send_sem.at[layer, 2])
-        all_of(drecv.at[layer, pl.ds(0, nz - 1)], send_sem.at[layer, 3])
-        pltpu.make_async_copy(mem_v.at[layer], mem_o.at[layer], out_sem.at[layer]).wait()
-    for copy in outs:
+
+
+def put_out(mixed_v, mem_v, nrm_v, stab_v, mixed_o, mem_o, nrm_o, stab_o, sem):
+    copies = [
+        pltpu.make_async_copy(mem_v, mem_o, sem.at[0]),
+        pltpu.make_async_copy(nrm_v, nrm_o, sem.at[1]),
+        pltpu.make_async_copy(stab_v, stab_o, sem.at[2]),
+        pltpu.make_async_copy(mixed_v, mixed_o, sem.at[3]),
+    ]
+    for copy in copies:
+        copy.start()
+    for copy in copies:
         copy.wait()
 
 
@@ -306,16 +366,19 @@
     hbm = pl.BlockSpec(memory_space=pltpu.HBM)
     memory = memory.reshape(2, ROWS, HEAD, HEAD)
     normalizer = normalizer.reshape(2, ROWS, HEAD)
+    wg = jnp.transpose(wg, (0, 2, 1))
+    bias = jnp.transpose(bias, (0, 2, 1))
+    stabilizer = jnp.transpose(stabilizer, (0, 2, 1))
     out = pl.pallas_call(
         functools.partial(kernel, ntp, ndp),
         out_shape=(
-            jax.ShapeDtypeStruct(tokens.shape, BF16),
-            jax.ShapeDtypeStruct(memory.shape, F32),
-            jax.ShapeDtypeStruct(normalizer.shape, F32),
-            jax.ShapeDtypeStruct(stabilizer.shape, F32),
+            pltpu.VMEM(tokens.shape, BF16),
+            pltpu.VMEM(memory.shape, F32),
+            pltpu.VMEM(normalizer.shape, F32),
+            pltpu.VMEM(stabilizer.shape, F32),
         ),
         in_specs=[hbm] * 12,
-        out_specs=(hbm,) * 4,
+        out_specs=(pl.BlockSpec(memory_space=pltpu.VMEM),) * 4,
         scratch_shapes=[
             pltpu.VMEM(tokens.shape, BF16),
             pltpu.VMEM(gain.shape, BF16),
@@ -327,29 +390,38 @@
             pltpu.VMEM(memory.shape, BF16),
             pltpu.VMEM(normalizer.shape, F32),
             pltpu.VMEM(stabilizer.shape, F32),
-            pltpu.VMEM((2, ntp, ROWS, 128), BF16),
+            pltpu.VMEM((ntp, ROWS, 128), BF16),
+            pltpu.VMEM((nz // 2, 2, 2, ROWS, 128), BF16),
             pltpu.VMEM((2, ndp, ROWS, 5 * HEAD), BF16),
             pltpu.VMEM((2, ndp, ROWS, 5 * HEAD), BF16),
             pltpu.VMEM((2, 2 * ndp, ROWS, 128), BF16),
-            pltpu.VMEM((2, nz, ROWS, 128), BF16),
-            pltpu.VMEM((2, nz, ROWS, 128), BF16),
+            pltpu.VMEM((nz // 2, 2, ROWS, 128), BF16),
+            pltpu.VMEM((nz, 2, ROWS, 128), BF16),
+            pltpu.VMEM((nz, ROWS, 128), BF16),
+            pltpu.VMEM((nz, ROWS, 128), BF16),
             pltpu.SemaphoreType.DMA((6,)),
             pltpu.SemaphoreType.DMA((4,)),
             pltpu.SemaphoreType.DMA,
             pltpu.SemaphoreType.DMA,
             pltpu.SemaphoreType.DMA((2,)),
-            pltpu.SemaphoreType.DMA((2,)),
             pltpu.SemaphoreType.DMA((2, 4)),
             pltpu.SemaphoreType.DMA((2, 4)),
+            pltpu.SemaphoreType.DMA((len(GROUPS),)),
         ],
         compiler_params=pltpu.CompilerParams(collective_id=0, has_side_effects=True),
     )(tokens, gain, wq, wk, wv, wo, wg, bias, wout, memory, normalizer, stabilizer)
-    mixed, new_memory, new_normalizer, new_stabilizer = out
+    mixed, new_memory, new_normalizer, new_stabilizer = pl.pallas_call(
+        put_out,
+        out_shape=tuple(jax.ShapeDtypeStruct(o.shape, o.dtype) for o in out),
+        in_specs=[pl.BlockSpec(memory_space=pltpu.VMEM)] * 4,
+        out_specs=(hbm,) * 4,
+        scratch_shapes=[pltpu.SemaphoreType.DMA((4,))],
+    )(*(pltpu.with_memory_space_constraint(o, pltpu.VMEM) for o in out))
     return (
         mixed,
         new_memory.reshape(2, ROWS, 1, HEAD, HEAD),
         new_normalizer.reshape(2, ROWS, 1, HEAD),
-        new_stabilizer,
+        jnp.transpose(new_stabilizer, (0, 2, 1)),
     )
 
 

time: 76.8 us -> 63.6 us (0.83)
  local copies, waits for them, and re-layouts: 8.47 us -> 0 us
  Pallas kernels: 67.4 us -> 62 us
    unnamed x17 -> x0, local copies, waits for them, and re-layouts: 8.47 us -> none
    pallas_call x1 -> x2, Pallas kernels: 67.4 us -> 62 us  [the longest x1 60.9 us: body(): pl.pallas_call(functools.partial(kernel, ntp, ndp), out_shape=(pltpu.VMEM...]
where the time goes in v2:
time: 63.6 us; the launch traced here: 62.6 us
  Pallas kernels  62 us (97%)
  between operations  0.64 us (1%)
    pallas_call x1, Pallas kernels, body(): pl.pallas_call(functools.partial(kernel, ntp, ndp), out_shape=(pltpu.VMEM...  60.9 us

profile of v2, /device:TPU:1, one launch (start us, length us, event | category | flops | bytes accessed | tf_op | source)
XLA Modules:
  0.0 62.6 jit_solution(2809784109362034537)
XLA Ops:
  0.6 60.9 %shard_map.147 = (bf16[4,256]{1,0:T(4,128)(2,1)S(1)}, f32[2,8,128,128]{3,2,1,0:T(8,128)S(1)}, f32[2,8,128]{2,1,0:T(8,128)S(1)}, f32[2,1,8]{2,1,0:T(1,128)S(1)}) custom-call(bf16[4,256]{1,0:T(4,128)(2,1)} %tok_h.1, bf16[2,256]{1,0:T(2,128)(2,1)} %gain_h.1, bf16[2,256,128]{2,1,0:T(8,128)(2,1)} %wq_h.1, bf16[2,256,128]{2,1,0:T(8,128)(2,1)} %wk_h.1, ...), custom_call_target="tpu_custom_call" | custom-call | tf_op jit(solution)/shard_map/pallas_call | solution.py:372
  61.6 1.0 %shard_map.148 = (bf16[4,256]{1,0:T(4,128)(2,1)}, f32[2,8,128,128]{3,2,1,0:T(8,128)}, f32[2,8,128]{2,1,0:T(8,128)}, f32[2,1,8]{2,1,0:T(1,128)}) custom-call(bf16[4,256]{1,0:T(4,128)(2,1)S(1)} %get-tuple-element.12.mixed_v, f32[2,8,128,128]{3,2,1,0:T(8,128)S(1)} %get-tuple-element.13.mem_v, f32[2,8,128]{2,1,0:T(8,128)S(1)} %get-tuple-element.14.nrm_v, ...), custom_call_target="tpu_custom_call" | custom-call | tf_op jit(solution)/shard_map/pallas_call | solution.py:413
